TPU v7x, 32 devices: a whole 2x2x4 slice. The times are simulated.
32 devices in a mesh: grp: 2 (over x), ep: 16 (over z, y, core).
Axes of the slice: x: 2, y: 2, z: 4, core: 2. Of those that a mesh axis runs over, the one named last changes fastest.
Arguments:
- tokens: bfloat16 [512, 2048], P(('grp', 'ep')), parts along dimension 0, may hold values from -6 to 6
- attn_gain: float32 [2048], replicated, may hold values from 0.1 to 1.9
- w_query: bfloat16 [2048, 1024], replicated, may hold values from -0.125 to 0.125
- w_key: bfloat16 [2048, 128], replicated, may hold values from -0.125 to 0.125
- w_value: bfloat16 [2048, 128], replicated, may hold values from -0.125 to 0.125
- w_forget: bfloat16 [2048, 2], replicated, may hold values from -0.125 to 0.125
- forget_bias: float32 [2], replicated, may hold values from -3 to 1
- w_attn_out: bfloat16 [1024, 2048], replicated, may hold values from -0.1875 to 0.1875
- cache_keys: bfloat16 [512, 1024, 128], P(('grp', 'ep')), parts along dimension 0, may hold values from -640 to 640
- cache_values: bfloat16 [512, 1024, 128], P(('grp', 'ep')), parts along dimension 0, may hold values from -6 to 6
- cache_logsum: float32 [512, 2, 1024], P(('grp', 'ep')), parts along dimension 0, may hold values from -100 to 0, as said below
- lengths: int32 [512], P(('grp', 'ep')), parts along dimension 0, may hold values from 1 to 1024, as said below
- ffn_gain: float32 [2048], replicated, may hold values from 0.1 to 1.9
- branch_gate: float32 [2048], replicated, may hold values from -0.125 to 0.125
- dense_gate: bfloat16 [2048, 4096], P(None, 'ep'), may hold values from -0.125 to 0.125
- dense_up: bfloat16 [2048, 4096], P(None, 'ep'), may hold values from -0.125 to 0.125
- dense_down: bfloat16 [4096, 2048], P('ep'), may hold values from -0.09375 to 0.09375
- expert_gate: bfloat16 [16, 2048, 512], P('ep'), may hold values from -0.125 to 0.125
- expert_up: bfloat16 [16, 2048, 512], P('ep'), may hold values from -0.125 to 0.125
- expert_down: bfloat16 [16, 512, 2048], P('ep'), may hold values from -0.25 to 0.25
- routes: int32 [512, 4], P(('grp', 'ep')), parts along dimension 0, may hold values from 0 to 15, all different within a row; in each aligned block of 16 rows (0 to 15, 16 to 31, ...) at most 8 rows name the same one
- route_weights: float32 [512, 4], P(('grp', 'ep')), parts along dimension 0, may hold values from 0.2 to 1
Outputs:
- output_rows: bfloat16 [512, 2048], P(('grp', 'ep')), parts along dimension 0
There are 2 independent parts, one for each index of `grp`. A program takes and returns all parts, laid end to end along the dimension named above; an argument that names none is the same for every part. Nothing has to cross between parts.
Inputs may be any that keep to these rules, and one draw needn't show every extreme that they name: `lengths`: each aligned block of 16 sequences holds one with 1024 valid positions; every length is at least 128. `routes`: a row's 4 experts differ; among the rows of one device no expert is named more than 8 times. `cache_logsum`: non-increasing along positions.
All inputs are finite; a program needn't handle non-finite values.
Results may differ from a plain program's by a relative error of at most 0.012.
The roundings to bfloat16 on the way count: a program that leaves them out, or rounds other values in their place, can miss the bound.
Values may be sent and summed in bfloat16 or wider, within the bound.
No kernel may reach another device: no remote copies, remote signals or barrier semaphores. Data moves between devices by JAX's collectives and lax.ppermute only.
A program may use at most 128 MiB of HBM per device.

v0:
```python
import math
import jax
import jax.numpy as jnp
from jax import lax
from jax.sharding import PartitionSpec as P

EPSILON = 1e-06


def norm_rows(inputs, gain_vec):
    widened = inputs.astype(jnp.float32)
    scaled = widened * lax.rsqrt(jnp.mean(widened * widened, axis=-1, keepdims=True) + EPSILON)
    return (scaled * gain_vec).astype(jnp.bfloat16)


def swiglu(row_block, w_first, w_second):
    gate_part = jnp.dot(row_block, w_first, preferred_element_type=jnp.float32)
    up_part = jnp.dot(row_block, w_second, preferred_element_type=jnp.float32)
    return (jax.nn.silu(gate_part) * up_part).astype(jnp.bfloat16)


def expert_rows(row_block, w_gate, w_up, w_down):
    middle = swiglu(row_block, w_gate, w_up)
    return jnp.dot(middle, w_down, preferred_element_type=jnp.float32).astype(jnp.bfloat16)


def attend(
    normed,
    w_query,
    w_key,
    w_value,
    w_forget,
    forget_bias,
    cache_keys,
    cache_values,
    cache_logsum,
    lengths,
):
    own_rows = normed.shape[0]
    kv_heads = cache_logsum.shape[1]
    cache_span = cache_logsum.shape[2]
    head_size = w_key.shape[1] // kv_heads
    group_size = w_query.shape[1] // head_size // kv_heads
    scaling = 1.0 / math.sqrt(head_size)
    queries = jnp.dot(normed, w_query, preferred_element_type=jnp.float32).astype(jnp.bfloat16)
    new_keys = jnp.dot(normed, w_key, preferred_element_type=jnp.float32).astype(jnp.bfloat16)
    new_values = jnp.dot(normed, w_value, preferred_element_type=jnp.float32).astype(jnp.bfloat16)
    log_gate = jax.nn.log_sigmoid(
        jnp.dot(normed, w_forget, preferred_element_type=jnp.float32) + forget_bias
    )
    positions = lax.broadcasted_iota(jnp.int32, (own_rows, kv_heads, cache_span), 2)
    latest = jnp.sum(jnp.where(positions == lengths[:, None, None] - 1, cache_logsum, 0.0), axis=2)
    offsets = (latest + log_gate)[:, :, None] - cache_logsum
    usable = positions < lengths[:, None, None]
    query_heads = queries.reshape(own_rows, kv_heads, group_size, head_size)
    key_heads = cache_keys.reshape(own_rows, cache_span, kv_heads, head_size)
    value_heads = cache_values.reshape(own_rows, cache_span, kv_heads, head_size)
    scores = (
        jnp.einsum("bgrd,blgd->bgrl", query_heads, key_heads, preferred_element_type=jnp.float32)
        * scaling
    )
    scores = jnp.where(usable[:, :, None, :], scores + offsets[:, :, None, :], -jnp.inf)
    self_score = (
        jnp.einsum(
            "bgrd,bgd->bgr",
            query_heads,
            new_keys.reshape(own_rows, kv_heads, head_size),
            preferred_element_type=jnp.float32,
        )
        * scaling
    )
    peak_score = jnp.maximum(jnp.max(scores, axis=3), self_score)
    cache_weight = jnp.exp(scores - peak_score[..., None])
    self_weight = jnp.exp(self_score - peak_score)
    denominator = jnp.sum(cache_weight, axis=3) + self_weight
    cache_probs = (cache_weight / denominator[..., None]).astype(jnp.bfloat16)
    self_probs = (self_weight / denominator).astype(jnp.bfloat16)
    attended = jnp.einsum(
        "bgrl,blgd->bgrd", cache_probs, value_heads, preferred_element_type=jnp.float32
    )
    attended = attended + self_probs.astype(jnp.float32)[..., None] * new_values.reshape(
        own_rows, kv_heads, 1, head_size
    ).astype(jnp.float32)
    return attended.reshape(own_rows, -1).astype(jnp.bfloat16)


def body(
    tokens,
    attn_gain,
    w_query,
    w_key,
    w_value,
    w_forget,
    forget_bias,
    w_attn_out,
    cache_keys,
    cache_values,
    cache_logsum,
    lengths,
    ffn_gain,
    branch_gate,
    dense_gate,
    dense_up,
    dense_down,
    expert_gate,
    expert_up,
    expert_down,
    routes,
    route_weights,
):
    own_rows = tokens.shape[0]
    normed = norm_rows(tokens, attn_gain)
    attended = attend(
        normed,
        w_query,
        w_key,
        w_value,
        w_forget,
        forget_bias,
        cache_keys,
        cache_values,
        cache_logsum,
        lengths,
    )
    residual = tokens.astype(jnp.float32) + jnp.dot(
        attended, w_attn_out, preferred_element_type=jnp.float32
    )
    second = norm_rows(residual, ffn_gain)
    branch_share = jax.nn.sigmoid(
        jnp.dot(second.astype(jnp.float32), branch_gate, precision=lax.Precision.HIGHEST)
    )
    expert_count = lax.axis_size("ep")
    route_count = routes.shape[1]
    capacity = max(2, 2 * own_rows * route_count // expert_count)
    hits = (
        routes[:, :, None]
        == lax.broadcasted_iota(jnp.int32, (own_rows, route_count, expert_count), 2)
    ).astype(jnp.int32)
    flat_hits = hits.reshape(own_rows * route_count, expert_count)
    order_rank = jnp.sum((jnp.cumsum(flat_hits, axis=0) - 1) * flat_hits, axis=1).reshape(
        own_rows, route_count
    )
    slot_index = routes * capacity + order_rank
    slot_total = expert_count * capacity
    matches = slot_index[None, :, :] == lax.broadcasted_iota(
        jnp.int32, (slot_total, own_rows, route_count), 0
    )
    dispatch = jnp.sum(matches.astype(jnp.float32), axis=2).astype(jnp.bfloat16)
    combine = jnp.sum(jnp.where(matches, route_weights[None, :, :], 0.0), axis=2).T
    outgoing = jnp.dot(dispatch, second, preferred_element_type=jnp.float32).astype(jnp.bfloat16)
    outgoing = outgoing.reshape(expert_count, 1, capacity, -1)
    arrived = lax.all_to_all(outgoing, "ep", split_axis=0, concat_axis=1, tiled=True)
    arrived_shape = arrived.shape
    answer = expert_rows(
        arrived.reshape(-1, arrived_shape[3]), expert_gate[0], expert_up[0], expert_down[0]
    )
    returned = lax.all_to_all(
        answer.reshape(arrived_shape), "ep", split_axis=1, concat_axis=0, tiled=True
    )
    routed = jnp.dot(
        combine,
        returned.reshape(slot_total, -1).astype(jnp.float32),
        precision=lax.Precision.HIGHEST,
    )
    dense_hidden = swiglu(lax.all_gather(second, "ep", axis=0, tiled=True), dense_gate, dense_up)
    dense = lax.psum_scatter(
        jnp.dot(dense_hidden, dense_down, preferred_element_type=jnp.float32).astype(jnp.bfloat16),
        "ep",
        scatter_dimension=0,
        tiled=True,
    ).astype(jnp.float32)
    output_rows = residual + branch_share[:, None] * dense + routed
    return output_rows.astype(jnp.bfloat16)


def solution(mesh):
    return jax.shard_map(
        body,
        mesh=mesh,
        in_specs=(
            P(("grp", "ep"), None),
            P(),
            P(),
            P(),
            P(),
            P(),
            P(),
            P(),
            P(("grp", "ep"), None, None),
            P(("grp", "ep"), None, None),
            P(("grp", "ep"), None, None),
            P(("grp", "ep")),
            P(),
            P(),
            P(None, "ep"),
            P(None, "ep"),
            P("ep", None),
            P("ep", None, None),
            P("ep", None, None),
            P("ep", None, None),
            P(("grp", "ep"), None),
            P(("grp", "ep"), None),
        ),
        out_specs=P(("grp", "ep"), None),
        check_vma=False,
    )
```

profile of v0, /device:TPU:0, one launch (start us, length us, event | category | flops | bytes accessed | tf_op | source)
XLA Modules:
  0.0 152.9 jit_solution(14952245672474803569)
XLA Ops:
  6.6 0.8 broadcast_add_fusion
  7.4 0.8 iota_compare_fusion
  8.2 1.0 fusion.43
  9.2 2.9 %convolution_convert_fusion.3 = bf16[16,1024]{1,0:T(8,128)(2,1)S(1)} fusion(bf16[2048,1024]{1,0:T(8,128)(2,1)} %param.24, bf16[16,2048]{1,0:T(8,128)(2,1)} %param.22, f32[2048]{0:T(1024)} %param.23, f32[16]{0:T(128)S(1)} %add_rsqrt_fusion.1), kind=kOutput, calls=%fused_computation.22 | convolution fusion | flops 67256320 | bytes 4300864 | tf_op jit(solution)/shard_map/dot_general | solution.py:45
  12.1 0.1 reshape.95
  12.3 0.2 fusion.46
  12.6 0.2 fusion.53
  12.9 0.1 broadcast_subtract_fusion
  13.0 6.5 %copy.53 = bf16[16,1024,128]{1,2,0:T(8,128)(2,1)} copy(bf16[16,1024,128]{2,1,0:T(8,128)(2,1)} %param.30) | data formatting | bytes 8388608 | tf_op args[8]
  19.5 0.2 convolution_convert_fusion.5
  19.8 0.2 fusion.62
  20.0 3.0 %fusion.61 = (f32[16,2,8]{2,1,0:T(2,128)S(1)}, f32[16,2,8,1024]{3,2,1,0:T(8,128)S(1)}) fusion(f32[16,2,1024]{2,1,0:T(2,128)S(1)} %broadcast_subtract_fusion, bf16[16,2,8,64]{3,2,1,0:T(8,128)(2,1)S(1)} %reshape.95, bf16[16,1024,2,64]{1,3,2,0:T(8,128)(2,1)} %bitcast.70, pred[16,2,1024]{2,1,0:T(4,128)(4,1)S(1)} %iota_compare_fusion), kind=kOutput, calls=%fused_computation.85 | convolution fusion | flops 34602752 | bytes 5440512 | tf_op jit(solution)/shard_map/bgrd,blgd->bgrl/dot_general | solution.py:59
  23.0 0.3 fusion.24
  23.3 1.3 fusion.18
  24.7 6.4 %copy.56 = bf16[16,1024,128]{1,2,0:T(8,128)(2,1)} copy(bf16[16,1024,128]{2,1,0:T(8,128)(2,1)} %param.31) | data formatting | bytes 8388608 | tf_op args[9]
  31.1 3.4 %fusion.17 = bf16[16,2,8,64]{3,2,1,0:T(8,128)(2,1)S(1)} fusion(bf16[16,1024,2,64]{1,3,2,0:T(8,128)(2,1)} %bitcast.71, f32[16,2,8,1024]{3,2,1,0:T(8,128)S(1)} %get-tuple-element.10, f32[16,2,8]{2,1,0:T(2,128)S(1)} %get-tuple-element.8, f32[16,2,8]{2,1,0:T(2,128)S(1)} %multiply_maximum_fusion, f32[16,2,64]{2,1,0:T(2,128)S(1)} %reshape.103, ...), kind=kOutput, calls=%fused_computation.21 | convolution fusion | flops 34390016 | bytes 5286912 | tf_op jit(solution)/shard_map/bgrl,blgd->bgrd/dot_general | solution.py:78
  34.5 0.1 convert_element_type.90
  34.7 3.0 %multiply_reduce_fusion = (f32[16]{0:T(128)S(1)}, f32[16,2048]{1,0:T(8,128)S(1)}) fusion(bf16[16,1024]{1,0:T(8,128)(2,1)S(1)} %convert_element_type.90, bf16[1024,2048]{1,0:T(8,128)(2,1)} %param.29, bf16[16,2048]{1,0:T(8,128)(2,1)S(1)} %copy-done.1), kind=kOutput, calls=%fused_computation.61 | convolution fusion | flops 67239920 | bytes 4423744 | tf_op jit(solution)/shard_map/dot_general | solution.py:125
  37.7 0.7 multiply_convert_fusion
  38.8 0.2 select_reduce_fusion.1
  39.2 2.0 %fusion = bf16[16,1,8,2048]{3,2,1,0:T(8,128)(2,1)} fusion(bf16[16,2048]{1,0:T(8,128)(2,1)} %multiply_convert_fusion, bf16[128,16]{0,1:T(8,128)(2,1)S(1)} %get-tuple-element.5), kind=kOutput, calls=%fused_computation.3 | convolution fusion | flops 8650752 | bytes 593920 | tf_op jit(solution)/shard_map/dot_general | solution.py:150
  41.2 7.4 %all-to-all-start = ((bf16[16,1,8,2048]{3,2,1,0:T(8,128)(2,1)}), bf16[16,1,8,2048]{3,2,1,0:T(8,128)(2,1)S(1)}, u32[]{:S(2)}, u32[]{:S(2)}) async-start(bf16[16,1,8,2048]{3,2,1,0:T(8,128)(2,1)} %fusion), calls=%async_computation.1 | async-start | bytes 1048576 | tf_op jit(solution)/shard_map/all_to_all | solution.py:152
  48.6 32.8 %all-gather.2.cloned.1.call-done = bf16[256,2048]{1,0:T(8,128)(2,1)} async-done(((bf16[16,2048]{1,0:T(8,128)(2,1)}), bf16[256,2048]{1,0:T(8,128)(2,1)}) %all-gather.2.cloned.1.call-update) | async-done | bytes 1048592 | tf_op jit(solution)/shard_map/all_gather | solution.py:165
  81.5 2.0 %fusion.63 = f32[256,256]{1,0:T(8,128)S(1)} fusion(bf16[256,2048]{1,0:T(8,128)(2,1)} %all-gather.2.cloned.1.call-done, bf16[2048,256]{1,0:T(8,128)(2,1)} %param.36), kind=kOutput, calls=%fused_computation.87 | convolution fusion | flops 268435456 | bytes 2359296 | tf_op jit(solution)/shard_map/dot_general | solution.py:17
  83.4 4.1 %convolution_convert_fusion = bf16[256,2048]{1,0:T(8,128)(2,1)} fusion(bf16[256,2048]{1,0:T(8,128)(2,1)} %param.38, bf16[256,2048]{1,0:T(8,128)(2,1)} %all-gather.2.cloned.1.call-done, bf16[2048,256]{1,0:T(8,128)(2,1)} %param.37, f32[256,256]{1,0:T(8,128)S(1)} %fusion.63), kind=kOutput, calls=%fused_computation | convolution fusion | flops 537788416 | bytes 4456448 | tf_op jit(solution)/shard_map/dot_general | solution.py:167
  87.6 2.0 %fusion.6 = f32[128,512]{1,0:T(8,128)S(1)} fusion(bf16[1,2048,512]{2,1,0:T(8,128)(2,1)} %param.39, bf16[16,1,8,2048]{3,2,1,0:T(8,128)(2,1)S(1)} %all-to-all-done), kind=kOutput, calls=%fused_computation.11 | convolution fusion | flops 268435456 | bytes 2883584 | tf_op jit(solution)/shard_map/dot_general | solution.py:17
  89.7 3.2 %fusion.1 = bf16[1,16,8,2048]{3,2,0,1:T(8,128)(2,1)} fusion(bf16[1,512,2048]{2,1,0:T(8,128)(2,1)S(1)} %copy-done, bf16[1,2048,512]{2,1,0:T(8,128)(2,1)} %param.40, bf16[16,1,8,2048]{3,2,1,0:T(8,128)(2,1)S(1)} %all-to-all-done, f32[128,512]{1,0:T(8,128)S(1)} %fusion.6), kind=kOutput, calls=%fused_computation.4 | convolution fusion | flops 537526272 | bytes 5505024 | tf_op jit(solution)/shard_map/dot_general | solution.py:24
  92.9 3.7 %all-to-all-start.1 = ((bf16[1,16,8,2048]{3,2,0,1:T(8,128)(2,1)}), bf16[1,16,8,2048]{3,2,0,1:T(8,128)(2,1)S(1)}, u32[]{:S(2)}, u32[]{:S(2)}) async-start(bf16[1,16,8,2048]{3,2,0,1:T(8,128)(2,1)} %fusion.1), calls=%async_computation.2 | async-start | bytes 1048576 | tf_op jit(solution)/shard_map/all_to_all | solution.py:157
  96.7 0.1 fusion.23
  96.8 14.1 %all-to-all-done.1 = bf16[1,16,8,2048]{3,2,0,1:T(8,128)(2,1)S(1)} async-done(((bf16[1,16,8,2048]{3,2,0,1:T(8,128)(2,1)}), bf16[1,16,8,2048]{3,2,0,1:T(8,128)(2,1)S(1)}, u32[]{:S(2)}, u32[]{:S(2)}) %all-to-all-start.1) | async-done | bytes 524320 | tf_op jit(solution)/shard_map/all_to_all | solution.py:157
  110.9 33.4 %reduce-scatter.2.cloned.1.call-done = bf16[16,2048]{1,0:T(8,128)(2,1)} async-done(((bf16[256,2048]{1,0:T(8,128)(2,1)}), bf16[16,2048]{1,0:T(8,128)(2,1)}) %reduce-scatter.2.cloned.1.call-update) | async-done | bytes 65552 | tf_op jit(solution)/shard_map/reduce_scatter | solution.py:166
  144.3 1.8 %fusion.2 = bf16[16,2048]{1,0:T(8,128)(2,1)} fusion(f32[128,16]{0,1:T(8,128)S(1)} %get-tuple-element.6, bf16[1,16,8,2048]{3,2,0,1:T(8,128)(2,1)S(1)} %all-to-all-done.1, f32[16,2048]{1,0:T(8,128)S(1)} %get-tuple-element.12, bf16[16,2048]{1,0:T(8,128)(2,1)} %reduce-scatter.2.cloned.1.call-done, f32[16]{0:T(128)S(1)} %fusion.23), kind=kOutput, calls=%fused_computation.7 | convolution fusion | flops 50495488 | bytes 794688 | tf_op jit(solution)/shard_map/dot_general | solution.py:160
  (45 shorter events, 1.2 us)
Async XLA Ops:
  6.5 83.2 %copy-start = (bf16[1,512,2048]{2,1,0:T(8,128)(2,1)S(1)}, bf16[1,512,2048]{2,1,0:T(8,128)(2,1)}, u32[]{:S(2)}) copy-start(bf16[1,512,2048]{2,1,0:T(8,128)(2,1)} %param.41) | copy-start | bytes 6291460
  6.5 6.0 %copy-start.1 = (bf16[16,2048]{1,0:T(8,128)(2,1)S(1)}, bf16[16,2048]{1,0:T(8,128)(2,1)}, u32[]{:S(2)}) copy-start(bf16[16,2048]{1,0:T(8,128)(2,1)} %param.22) | copy-start | bytes 196612
  6.5 6.0 %copy-start.5 = (f32[2048]{0:T(1024)S(1)}, f32[2048]{0:T(1024)}, u32[]{:S(2)}) copy-start(f32[2048]{0:T(1024)} %param.23) | copy-start | bytes 24580
  6.5 5.7 %copy-start.4 = (f32[16,2,1024]{2,1,0:T(2,128)S(1)}, f32[16,2,1024]{2,1,0:T(2,128)}, u32[]{:S(2)}) copy-start(f32[16,2,1024]{2,1,0:T(2,128)} %param.32) | copy-start | bytes 393220
  6.5 6.0 %copy-start.9 = (bf16[2048,2]{0,1:T(2,128)(2,1)S(1)}, bf16[2048,2]{0,1:T(2,128)(2,1)}, u32[]{:S(2)}) copy-start(bf16[2048,2]{0,1:T(2,128)(2,1)} %param.27) | copy-start | bytes 24580
  6.5 6.0 %copy-start.11 = (f32[2]{0:T(128)S(1)}, f32[2]{0:T(128)}, u32[]{:S(2)}) copy-start(f32[2]{0:T(128)} %param.28) | copy-start | bytes 28
  6.6 74.9 %all-gather.2.cloned.1.call-start = ((), (), s32[]{:S(2)}) async-start(), calls=%async_computation.3 | async-start | bytes 1114112 | tf_op jit(solution)/shard_map/all_gather | solution.py:165
  13.0 6.5 %copy-start.3 = (bf16[2048,128]{1,0:T(8,128)(2,1)S(1)}, bf16[2048,128]{1,0:T(8,128)(2,1)}, u32[]{:S(2)}) copy-start(bf16[2048,128]{1,0:T(8,128)(2,1)} %param.25) | copy-start | bytes 1572868
  31.1 6.6 %copy-start.6 = (f32[2048]{0:T(1024)S(1)}, f32[2048]{0:T(1024)}, u32[]{:S(2)}) copy-start(f32[2048]{0:T(1024)} %param.34) | copy-start | bytes 24580
  34.5 3.9 %copy-start.7 = (s32[16,4]{0,1:T(4,128)S(1)}, s32[16,4]{0,1:T(4,128)}, u32[]{:S(2)}) copy-start(s32[16,4]{0,1:T(4,128)} %param.42) | copy-start | bytes 772
  34.5 4.6 %copy-start.8 = (f32[16,4]{0,1:T(4,128)S(1)}, f32[16,4]{0,1:T(4,128)}, u32[]{:S(2)}) copy-start(f32[16,4]{0,1:T(4,128)} %param.43) | copy-start | bytes 772
  41.2 46.4 %all-to-all-start = ((bf16[16,1,8,2048]{3,2,1,0:T(8,128)(2,1)}), bf16[16,1,8,2048]{3,2,1,0:T(8,128)(2,1)S(1)}, u32[]{:S(2)}, u32[]{:S(2)}) async-start(bf16[16,1,8,2048]{3,2,1,0:T(8,128)(2,1)} %fusion), calls=%async_computation.1 | async-start | bytes 1048576 | tf_op jit(solution)/shard_map/all_to_all | solution.py:152
  48.6 95.7 %reduce-scatter.2.cloned.1.call-start = ((), (), s32[]{:S(2)}) async-start(), calls=%async_computation.4 | async-start | bytes 1114112 | tf_op jit(solution)/shard_map/reduce_scatter | solution.py:166
  87.6 9.0 %copy-start.2 = (bf16[16,2048]{1,0:T(8,128)(2,1)S(1)}, bf16[16,2048]{1,0:T(8,128)(2,1)}, u32[]{:S(2)}) copy-start(bf16[16,2048]{1,0:T(8,128)(2,1)} %multiply_convert_fusion) | copy-start | bytes 196612
  87.6 9.0 %copy-start.10 = (f32[2048]{0:T(1024)S(1)}, f32[2048]{0:T(1024)}, u32[]{:S(2)}) copy-start(f32[2048]{0:T(1024)} %param.35) | copy-start | bytes 24580
  92.9 18.0 %all-to-all-start.1 = ((bf16[1,16,8,2048]{3,2,0,1:T(8,128)(2,1)}), bf16[1,16,8,2048]{3,2,0,1:T(8,128)(2,1)S(1)}, u32[]{:S(2)}, u32[]{:S(2)}) async-start(bf16[1,16,8,2048]{3,2,0,1:T(8,128)(2,1)} %fusion.1), calls=%async_computation.2 | async-start | bytes 1048576 | tf_op jit(solution)/shard_map/all_to_all | solution.py:157
Sparse Core Ops, SparseCore 0:
  38.5 42.8 all-gather.1
  87.7 56.5 reduce-scatter.1
where the time goes:
time: 154 us; the launch traced here: 153 us
  waiting for transfers between devices  80.4 us (52%)
  matrix products  29.5 us (19%)
  local copies, waits for them, and re-layouts  13.8 us (9%)
  between operations  13.6 us (9%)
  starting transfers between devices  11.2 us (7%)
  other arithmetic  4.46 us (3%)
    reduce_scatter x1, waiting for transfers between devices, body(): lax.psum_scatter(jnp.dot(dense_hidden, dense_down, preferred_element_type...  33.4 us
    all_gather x1, waiting for transfers between devices, body(): lax.all_gather(second, 'ep', axis=0, tiled=True)  32.8 us
    all_to_all x1, waiting for transfers between devices, body(): lax.all_to_all(answer.reshape(arrived_shape), 'ep', split_axis=1, concat_...  14.1 us
    unnamed x27, local copies, waits for them, and re-layouts  13 us
    all_to_all x1, starting transfers between devices, body(): lax.all_to_all(outgoing, 'ep', split_axis=0, concat_axis=1, tiled=True)  7.41 us
    dot_general x1, matrix products, body(): jnp.dot(dense_hidden, dense_down, preferred_element_type=jnp.float32)  4.14 us
    dot_general x2, matrix products, swiglu(): gate_part = jnp.dot(row_block, w_first, preferred_element_type=jnp.float32)  4.02 us
    all_to_all x1, starting transfers between devices, body(): lax.all_to_all(answer.reshape(arrived_shape), 'ep', split_axis=1, concat_...  3.68 us
  transfers between devices with their start and end apart: 4, of which 3 were waited for; matrix products, arithmetic and copies ran while one was open for 9% of the time, Pallas kernels for 0%

commit v1 on v0

--- a/solution.py
+++ b/solution.py
@@ -154,8 +154,14 @@
     answer = expert_rows(
         arrived.reshape(-1, arrived_shape[3]), expert_gate[0], expert_up[0], expert_down[0]
     )
-    returned = lax.all_to_all(
-        answer.reshape(arrived_shape), "ep", split_axis=1, concat_axis=0, tiled=True
+    returned = jnp.concatenate(
+        lax.all_to_all(
+            jnp.stack(jnp.split(answer.reshape(arrived_shape), lax.axis_size("ep"), axis=1)),
+            "ep",
+            0,
+            0,
+        ),
+        axis=0,
     )
     routed = jnp.dot(
         combine,

time: 154 us -> 162 us (1.052)
  local copies, waits for them, and re-layouts: 13.8 us -> 23.5 us
    all_gather x1, waiting for transfers between devices: 32.8 us -> 14.2 us  [body(): lax.all_gather(second, 'ep', axis=0, tiled=True)]
    all_to_all x1, waiting for transfers between devices: 0.01 us -> 13.5 us  [body(): lax.all_to_all(outgoing, 'ep', split_axis=0, concat_axis=1, tiled=True)]
    unnamed x27 -> x44, local copies, waits for them, and re-layouts: 13 us -> 22.1 us
    reduce_scatter x1, waiting for transfers between devices: 33.4 us -> 37.5 us  [body(): lax.psum_scatter(jnp.dot(dense_hidden, dense_down, preferred_element_type...]
  transfers between devices with their start and end apart: 4 -> 4, of which waited for: 3 -> 4; matrix products, arithmetic and copies ran while one was open for 9% -> 9% of each run, Pallas kernels for 0% -> 0%
where the time goes in v1:
time: 162 us; the launch traced here: 161 us
  waiting for transfers between devices  80 us (49%)
  matrix products  28.6 us (18%)
  local copies, waits for them, and re-layouts  23.5 us (15%)
  between operations  13.6 us (8%)
  starting transfers between devices  11.2 us (7%)
  other arithmetic  3.86 us (2%)
    reduce_scatter x1, waiting for transfers between devices, body(): lax.psum_scatter(jnp.dot(dense_hidden, dense_down, preferred_element_type...  37.5 us
    unnamed x44, local copies, waits for them, and re-layouts  22.1 us
    all_gather x1, waiting for transfers between devices, body(): lax.all_gather(second, 'ep', axis=0, tiled=True)  14.2 us
    all_to_all x1, waiting for transfers between devices, body(): lax.all_to_all(jnp.stack(jnp.split(answer.reshape(arrived_shape), lax.axi...  14.1 us
    all_to_all x1, waiting for transfers between devices, body(): lax.all_to_all(outgoing, 'ep', split_axis=0, concat_axis=1, tiled=True)  13.5 us
    all_to_all x1, starting transfers between devices, body(): lax.all_to_all(outgoing, 'ep', split_axis=0, concat_axis=1, tiled=True)  7.41 us
    dot_general x2, matrix products, swiglu(): gate_part = jnp.dot(row_block, w_first, preferred_element_type=jnp.float32)  4.74 us
    dot_general x1, matrix products, body(): jnp.dot(dense_hidden, dense_down, preferred_element_type=jnp.float32)  4.18 us
  transfers between devices with their start and end apart: 4, of which 4 were waited for; matrix products, arithmetic and copies ran while one was open for 9% of the time, Pallas kernels for 0%

profile of v1, /device:TPU:0, one launch (start us, length us, event | category | flops | bytes accessed | tf_op | source)
XLA Modules:
  0.0 160.9 jit_solution(1650019868767233131)
XLA Ops:
  6.6 0.8 broadcast_add_fusion
  7.4 0.8 iota_compare_fusion
  8.2 1.0 fusion.43
  9.2 2.9 %convolution_convert_fusion.3 = bf16[16,1024]{1,0:T(8,128)(2,1)S(1)} fusion(bf16[2048,1024]{1,0:T(8,128)(2,1)} %param.24, bf16[16,2048]{1,0:T(8,128)(2,1)} %param.22, f32[2048]{0:T(1024)} %param.23, f32[16]{0:T(128)S(1)} %add_rsqrt_fusion.1), kind=kOutput, calls=%fused_computation.22 | convolution fusion | flops 67256320 | bytes 4300864 | tf_op jit(solution)/shard_map/dot_general | solution.py:45
  13.0 6.5 %copy.51 = bf16[16,1024,128]{1,2,0:T(8,128)(2,1)} copy(bf16[16,1024,128]{2,1,0:T(8,128)(2,1)} %param.30) | data formatting | bytes 8388608 | tf_op args[8]
  20.0 3.0 %fusion.61 = (f32[16,2,8]{2,1,0:T(2,128)S(1)}, f32[16,2,8,1024]{3,2,1,0:T(8,128)S(1)}) fusion(f32[16,2,1024]{2,1,0:T(2,128)S(1)} %broadcast_subtract_fusion, bf16[16,2,8,64]{3,2,1,0:T(8,128)(2,1)S(1)} %reshape.88, bf16[16,1024,2,64]{1,3,2,0:T(8,128)(2,1)} %bitcast.132, pred[16,2,1024]{2,1,0:T(4,128)(4,1)S(1)} %iota_compare_fusion), kind=kOutput, calls=%fused_computation.117 | convolution fusion | flops 34602752 | bytes 5440512 | tf_op jit(solution)/shard_map/bgrd,blgd->bgrl/dot_general | solution.py:59
  23.3 1.3 fusion.18
  24.7 6.4 %copy.54 = bf16[16,1024,128]{1,2,0:T(8,128)(2,1)} copy(bf16[16,1024,128]{2,1,0:T(8,128)(2,1)} %param.31) | data formatting | bytes 8388608 | tf_op args[9]
  31.1 3.5 %fusion.17 = bf16[16,2,8,64]{3,2,1,0:T(8,128)(2,1)S(1)} fusion(bf16[16,1024,2,64]{1,3,2,0:T(8,128)(2,1)} %bitcast.133, f32[16,2,8,1024]{3,2,1,0:T(8,128)S(1)} %get-tuple-element.10, f32[16,2,8]{2,1,0:T(2,128)S(1)} %get-tuple-element.8, f32[16,2,8]{2,1,0:T(2,128)S(1)} %multiply_maximum_fusion, f32[16,2,64]{2,1,0:T(2,128)S(1)} %reshape.95, ...), kind=kOutput, calls=%fused_computation.21 | convolution fusion | flops 34390016 | bytes 5286912 | tf_op jit(solution)/shard_map/bgrl,blgd->bgrd/dot_general | solution.py:78
  34.7 3.0 %multiply_reduce_fusion = (f32[16]{0:T(128)S(1)}, f32[16,2048]{1,0:T(8,128)S(1)}) fusion(bf16[16,1024]{1,0:T(8,128)(2,1)S(1)} %convert_element_type.90, bf16[1024,2048]{1,0:T(8,128)(2,1)} %param.29, bf16[16,2048]{1,0:T(8,128)(2,1)S(1)} %copy-done.1), kind=kOutput, calls=%fused_computation.61 | convolution fusion | flops 67239920 | bytes 4423744 | tf_op jit(solution)/shard_map/dot_general | solution.py:125
  38.6 1.1 fusion
  39.7 7.4 %all-to-all-start = ((bf16[16,1,8,2048]{3,2,1,0:T(8,128)(2,1)}), bf16[16,1,8,2048]{3,2,1,0:T(8,128)(2,1)S(1)}, u32[]{:S(2)}, u32[]{:S(2)}) async-start(bf16[16,1,8,2048]{3,2,1,0:T(8,128)(2,1)} %fusion), calls=%async_computation.1 | async-start | bytes 1048576 | tf_op jit(solution)/shard_map/all_to_all | solution.py:152
  47.2 0.7 all-gather.2.cloned.1.call-update
  47.9 13.5 %all-to-all-done = bf16[16,1,8,2048]{3,2,1,0:T(8,128)(2,1)S(1)} async-done(((bf16[16,1,8,2048]{3,2,1,0:T(8,128)(2,1)}), bf16[16,1,8,2048]{3,2,1,0:T(8,128)(2,1)S(1)}, u32[]{:S(2)}, u32[]{:S(2)}) %all-to-all-start) | async-done | bytes 524320 | tf_op jit(solution)/shard_map/all_to_all | solution.py:152
  61.4 2.8 %fusion.6 = f32[128,512]{1,0:T(8,128)} fusion(bf16[1,2048,512]{2,1,0:T(8,128)(2,1)} %param.39, bf16[16,1,8,2048]{3,2,1,0:T(8,128)(2,1)S(1)} %all-to-all-done), kind=kOutput, calls=%fused_computation.11 | convolution fusion | flops 268435456 | bytes 2883584 | tf_op jit(solution)/shard_map/dot_general | solution.py:17
  64.2 2.4 %fusion.1 = bf16[1,16,8,2048]{3,2,1,0:T(8,128)(2,1)S(1)} fusion(bf16[1,512,2048]{2,1,0:T(8,128)(2,1)S(1)} %copy-done, bf16[1,2048,512]{2,1,0:T(8,128)(2,1)} %param.40, bf16[16,1,8,2048]{3,2,1,0:T(8,128)(2,1)S(1)} %all-to-all-done, f32[128,512]{1,0:T(8,128)} %fusion.6), kind=kOutput, calls=%fused_computation.4 | convolution fusion | flops 537526272 | bytes 5505024 | tf_op jit(solution)/shard_map/dot_general | solution.py:24
  66.6 0.6 constant_dynamic-update-slice_fusion.15
  67.2 0.6 constant_dynamic-update-slice_fusion.14
  69.7 0.6 constant_dynamic-update-slice_fusion.10
  70.3 0.6 constant_dynamic-update-slice_fusion.9
  70.9 0.6 constant_dynamic-update-slice_fusion.8
  72.1 0.6 constant_dynamic-update-slice_fusion.6
  74.5 0.6 constant_dynamic-update-slice_fusion.2
  75.1 14.2 %all-gather.2.cloned.1.call-done = bf16[256,2048]{1,0:T(8,128)(2,1)} async-done(((bf16[16,2048]{1,0:T(8,128)(2,1)}), bf16[256,2048]{1,0:T(8,128)(2,1)}) %all-gather.2.cloned.1.call-update) | async-done | bytes 1048592 | tf_op jit(solution)/shard_map/all_gather | solution.py:171
  89.4 2.0 %fusion.63 = f32[256,256]{1,0:T(8,128)S(1)} fusion(bf16[256,2048]{1,0:T(8,128)(2,1)} %all-gather.2.cloned.1.call-done, bf16[2048,256]{1,0:T(8,128)(2,1)} %param.36), kind=kOutput, calls=%fused_computation.119 | convolution fusion | flops 268435456 | bytes 2359296 | tf_op jit(solution)/shard_map/dot_general | solution.py:17
  91.3 4.2 %convolution_convert_fusion = bf16[256,2048]{1,0:T(8,128)(2,1)} fusion(bf16[256,2048]{1,0:T(8,128)(2,1)} %param.38, bf16[256,2048]{1,0:T(8,128)(2,1)} %all-gather.2.cloned.1.call-done, bf16[2048,256]{1,0:T(8,128)(2,1)} %param.37, f32[256,256]{1,0:T(8,128)S(1)} %fusion.63), kind=kOutput, calls=%fused_computation | convolution fusion | flops 537788416 | bytes 4456448 | tf_op jit(solution)/shard_map/dot_general | solution.py:173
  95.5 0.6 constant_dynamic-update-slice_fusion.1
  96.1 0.6 constant_dynamic-update-slice_fusion
  96.7 3.7 %all-to-all-start.1 = ((bf16[16,1,1,8,2048]{4,3,2,1,0:T(8,128)(2,1)}), bf16[16,1,1,8,2048]{4,3,2,1,0:T(8,128)(2,1)S(1)}, u32[]{:S(2)}, u32[]{:S(2)}) async-start(bf16[16,1,1,8,2048]{4,3,2,1,0:T(8,128)(2,1)} %constant_dynamic-update-slice_fusion), calls=%async_computation.2 | async-start | bytes 1048576 | tf_op jit(solution)/shard_map/all_to_all | solution.py:158
  100.6 14.1 %all-to-all-done.1 = bf16[16,1,1,8,2048]{4,3,2,1,0:T(8,128)(2,1)S(1)} async-done(((bf16[16,1,1,8,2048]{4,3,2,1,0:T(8,128)(2,1)}), bf16[16,1,1,8,2048]{4,3,2,1,0:T(8,128)(2,1)S(1)}, u32[]{:S(2)}, u32[]{:S(2)}) %all-to-all-start.1) | async-done | bytes 524320 | tf_op jit(solution)/shard_map/all_to_all | solution.py:158
  114.7 37.5 %reduce-scatter.2.cloned.1.call-done = bf16[16,2048]{1,0:T(8,128)(2,1)} async-done(((bf16[256,2048]{1,0:T(8,128)(2,1)}), bf16[16,2048]{1,0:T(8,128)(2,1)}) %reduce-scatter.2.cloned.1.call-update) | async-done | bytes 65552 | tf_op jit(solution)/shard_map/reduce_scatter | solution.py:172
  152.2 1.8 %fusion.2 = bf16[16,2048]{1,0:T(8,128)(2,1)} fusion(f32[128,16]{0,1:T(8,128)S(1)} %get-tuple-element.6, bf16[16,1,1,8,2048]{4,3,2,1,0:T(8,128)(2,1)S(1)} %all-to-all-done.1, f32[16,2048]{1,0:T(8,128)S(1)} %get-tuple-element.12, bf16[16,2048]{1,0:T(8,128)(2,1)} %reduce-scatter.2.cloned.1.call-done, f32[16]{0:T(128)S(1)} %fusion.23), kind=kOutput, calls=%fused_computation.7 | convolution fusion | flops 50495488 | bytes 794688 | tf_op jit(solution)/shard_map/dot_general | solution.py:166
  (63 shorter events, 7.3 us)
Async XLA Ops:
  6.5 57.7 %copy-start = (bf16[1,512,2048]{2,1,0:T(8,128)(2,1)S(1)}, bf16[1,512,2048]{2,1,0:T(8,128)(2,1)}, u32[]{:S(2)}) copy-start(bf16[1,512,2048]{2,1,0:T(8,128)(2,1)} %param.41) | copy-start | bytes 6291460
  6.5 6.0 %copy-start.1 = (bf16[16,2048]{1,0:T(8,128)(2,1)S(1)}, bf16[16,2048]{1,0:T(8,128)(2,1)}, u32[]{:S(2)}) copy-start(bf16[16,2048]{1,0:T(8,128)(2,1)} %param.22) | copy-start | bytes 196612
  6.5 6.0 %copy-start.6 = (f32[2048]{0:T(1024)S(1)}, f32[2048]{0:T(1024)}, u32[]{:S(2)}) copy-start(f32[2048]{0:T(1024)} %param.23) | copy-start | bytes 24580
  6.5 5.7 %copy-start.5 = (f32[16,2,1024]{2,1,0:T(2,128)S(1)}, f32[16,2,1024]{2,1,0:T(2,128)}, u32[]{:S(2)}) copy-start(f32[16,2,1024]{2,1,0:T(2,128)} %param.32) | copy-start | bytes 393220
  6.5 6.0 %copy-start.10 = (bf16[2048,2]{0,1:T(2,128)(2,1)S(1)}, bf16[2048,2]{0,1:T(2,128)(2,1)}, u32[]{:S(2)}) copy-start(bf16[2048,2]{0,1:T(2,128)(2,1)} %param.27) | copy-start | bytes 24580
  6.5 6.0 %copy-start.12 = (f32[2]{0:T(128)S(1)}, f32[2]{0:T(128)}, u32[]{:S(2)}) copy-start(f32[2]{0:T(128)} %param.28) | copy-start | bytes 28
  13.0 6.5 %copy-start.4 = (bf16[2048,128]{1,0:T(8,128)(2,1)S(1)}, bf16[2048,128]{1,0:T(8,128)(2,1)}, u32[]{:S(2)}) copy-start(bf16[2048,128]{1,0:T(8,128)(2,1)} %param.25) | copy-start | bytes 1572868
  31.1 6.6 %copy-start.8 = (s32[16,4]{0,1:T(4,128)S(1)}, s32[16,4]{0,1:T(4,128)}, u32[]{:S(2)}) copy-start(s32[16,4]{0,1:T(4,128)} %param.42) | copy-start | bytes 772
  31.1 7.3 %copy-start.9 = (f32[16,4]{0,1:T(4,128)S(1)}, f32[16,4]{0,1:T(4,128)}, u32[]{:S(2)}) copy-start(f32[16,4]{0,1:T(4,128)} %param.43) | copy-start | bytes 772
  31.1 7.4 %copy-start.7 = (f32[2048]{0:T(1024)S(1)}, f32[2048]{0:T(1024)}, u32[]{:S(2)}) copy-start(f32[2048]{0:T(1024)} %param.34) | copy-start | bytes 24580
  38.6 8.6 %copy-start.2 = (bf16[16,2048]{1,0:T(8,128)(2,1)}, bf16[16,2048]{1,0:T(8,128)(2,1)S(1)}, u32[]{:S(2)}) copy-start(bf16[16,2048]{1,0:T(8,128)(2,1)S(1)} %multiply_convert_fusion) | copy-start | bytes 196612
  39.7 21.7 %all-to-all-start = ((bf16[16,1,8,2048]{3,2,1,0:T(8,128)(2,1)}), bf16[16,1,8,2048]{3,2,1,0:T(8,128)(2,1)S(1)}, u32[]{:S(2)}, u32[]{:S(2)}) async-start(bf16[16,1,8,2048]{3,2,1,0:T(8,128)(2,1)} %fusion), calls=%async_computation.1 | async-start | bytes 1048576 | tf_op jit(solution)/shard_map/all_to_all | solution.py:152
  47.2 42.2 %all-gather.2.cloned.1.call-start = ((), (), s32[]{:S(2)}) async-start(), calls=%async_computation.3 | async-start | bytes 1114112 | tf_op jit(solution)/shard_map/all_gather | solution.py:171
  47.9 104.3 %reduce-scatter.2.cloned.1.call-start = ((), (), s32[]{:S(2)}) async-start(), calls=%async_computation.4 | async-start | bytes 1114112 | tf_op jit(solution)/shard_map/reduce_scatter | solution.py:172
  75.1 25.3 %copy-start.3 = (bf16[16,2048]{1,0:T(8,128)(2,1)S(1)}, bf16[16,2048]{1,0:T(8,128)(2,1)}, u32[]{:S(2)}) copy-start(bf16[16,2048]{1,0:T(8,128)(2,1)} %copy-done.2) | copy-start | bytes 196612
  75.1 25.3 %copy-start.11 = (f32[2048]{0:T(1024)S(1)}, f32[2048]{0:T(1024)}, u32[]{:S(2)}) copy-start(f32[2048]{0:T(1024)} %param.35) | copy-start | bytes 24580
  96.7 18.0 %all-to-all-start.1 = ((bf16[16,1,1,8,2048]{4,3,2,1,0:T(8,128)(2,1)}), bf16[16,1,1,8,2048]{4,3,2,1,0:T(8,128)(2,1)S(1)}, u32[]{:S(2)}, u32[]{:S(2)}) async-start(bf16[16,1,1,8,2048]{4,3,2,1,0:T(8,128)(2,1)} %constant_dynamic-update-slice_fusion), calls=%async_computation.2 | async-start | bytes 1048576 | tf_op jit(solution)/shard_map/all_to_all | solution.py:158
Sparse Core Ops, SparseCore 0:
  50.1 39.1 all-gather.1
  95.7 56.5 reduce-scatter.1
